TPU v7x, 32 devices: a whole 2x2x4 slice. The times are simulated.
32 devices in a mesh: rep: 4 (over y, x), fs: 2 (over core), tp: 4 (over z).
Axes of the slice: x: 2, y: 2, z: 4, core: 2. Of those that a mesh axis runs over, the one named last changes fastest.
Arguments:
- layer_input: bfloat16 [10240, 2048], P(('rep', 'fs'), 'tp'), may hold values from -6 to 6
- cotangent: bfloat16 [10240, 2048], P(('rep', 'fs'), 'tp'), may hold values from -8 to 8
- gate_pre: bfloat16 [10240, 3072], P('rep', 'fs'), may hold values from -8 to 8
- up_pre: bfloat16 [10240, 3072], P('rep', 'fs'), may hold values from -6 to 6
- gate_weight: bfloat16 [2048, 3072], P('tp', 'fs'), may hold values from -0.125 to 0.125
- up_weight: bfloat16 [2048, 3072], P('tp', 'fs'), may hold values from -0.125 to 0.125
- down_weight: bfloat16 [3072, 2048], P('fs', 'tp'), may hold values from -0.109375 to 0.109375
Outputs:
- input_grad: bfloat16 [10240, 2048], P(('rep', 'fs'), 'tp')
- gate_grad: float32 [2048, 3072], P('tp', 'fs')
- up_grad: float32 [2048, 3072], P('tp', 'fs')
- down_grad: float32 [3072, 2048], P('fs', 'tp')
- gate_rows_sq: float32 [2048], P('tp')
- up_rows_sq: float32 [2048], P('tp')
- down_rows_sq: float32 [3072], P('fs')
All inputs are finite; a program needn't handle non-finite values.
Results may differ from a plain program's by a relative error of at most 0.019.
Values may be sent and summed in bfloat16 or wider, within the bound.
No kernel may reach another device: no remote copies, remote signals or barrier semaphores. Data moves between devices by JAX's collectives and lax.ppermute only.
A program may use at most 128 MiB of HBM per device.

v0:
```python
import math

import jax
import jax.numpy as jnp
from jax import lax
from jax.sharding import PartitionSpec as P


def contract_rows(left_side, right_side):
    return lax.dot_general(
        left_side, right_side, (((0,), (0,)), ((), ())), preferred_element_type=jnp.float32
    )


def contract_cols(left_side, right_side):
    return lax.dot_general(
        left_side, right_side, (((1,), (1,)), ((), ())), preferred_element_type=jnp.float32
    )


def row_squares(gate_grad, up_grad, down_grad):
    gate_sq = jnp.sum(gate_grad * gate_grad, axis=1)
    up_sq = jnp.sum(up_grad * up_grad, axis=1)
    down_sq = jnp.sum(down_grad * down_grad, axis=1)
    gate_sq, up_sq = lax.psum((gate_sq, up_sq), "fs")
    down_sq = lax.psum(down_sq, "tp")
    return (gate_sq, up_sq, down_sq)


def on_device(layer_input, cotangent, gate_pre, up_pre, gate_weight, up_weight, down_weight):
    group_input, group_cotangent = (
        lax.all_gather(layer_input, "fs", axis=0, tiled=True),
        lax.all_gather(cotangent, "fs", axis=0, tiled=True),
    )
    hidden_grad = lax.psum(
        contract_cols(group_cotangent, down_weight).astype(jnp.bfloat16), "tp"
    ).astype(jnp.float32)
    gate_value = gate_pre.astype(jnp.float32)
    up_value = up_pre.astype(jnp.float32)
    sigmoid_gate = jax.nn.sigmoid(gate_value)
    activated = gate_value * sigmoid_gate
    hidden = (activated * up_value).astype(jnp.bfloat16)
    gate_delta = (
        hidden_grad * up_value * sigmoid_gate * (1.0 + gate_value * (1.0 - sigmoid_gate))
    ).astype(jnp.bfloat16)
    up_delta = (hidden_grad * activated).astype(jnp.bfloat16)
    input_grad = lax.psum_scatter(
        (contract_cols(gate_delta, gate_weight) + contract_cols(up_delta, up_weight)).astype(
            jnp.bfloat16
        ),
        "fs",
        scatter_dimension=0,
        tiled=True,
    )
    grad_scale = 1.0 / math.sqrt(group_input.shape[0] * lax.axis_size("rep"))
    gate_grad = contract_rows(group_input, gate_delta) * grad_scale
    up_grad = contract_rows(group_input, up_delta) * grad_scale
    down_grad = contract_rows(hidden, group_cotangent) * grad_scale
    gate_grad, up_grad, down_grad = (
        lax.psum(gate_grad.astype(jnp.bfloat16), "rep").astype(jnp.float32),
        lax.psum(up_grad.astype(jnp.bfloat16), "rep").astype(jnp.float32),
        lax.psum(down_grad.astype(jnp.bfloat16), "rep").astype(jnp.float32),
    )
    gate_sq, up_sq, down_sq = row_squares(gate_grad, up_grad, down_grad)
    return (input_grad, gate_grad, up_grad, down_grad, gate_sq, up_sq, down_sq)


def solution(mesh):
    return jax.shard_map(
        on_device,
        mesh=mesh,
        in_specs=(
            P(("rep", "fs"), "tp"),
            P(("rep", "fs"), "tp"),
            P("rep", "fs"),
            P("rep", "fs"),
            P("tp", "fs"),
            P("tp", "fs"),
            P("fs", "tp"),
        ),
        out_specs=(
            P(("rep", "fs"), "tp"),
            P("tp", "fs"),
            P("tp", "fs"),
            P("fs", "tp"),
            P("tp"),
            P("tp"),
            P("fs"),
        ),
        check_vma=False,
    )
```

profile of v0, /device:TPU:0, one launch (start us, length us, event | category | flops | bytes accessed | tf_op | source)
XLA Modules:
  0.0 484.3 jit_solution(10853355649280223357)
XLA Ops:
  7.2 0.0 all-gather.3.cloned.1.call-start
  7.2 0.7 all-gather.3.cloned.1.call-update
  7.9 0.0 all-reduce.5.cloned.1.call-start
  8.0 15.7 %all-gather.3.cloned.1.call-done = bf16[2560,512]{1,0:T(8,128)(2,1)} async-done(((bf16[1280,512]{1,0:T(8,128)(2,1)}), bf16[2560,512]{1,0:T(8,128)(2,1)}) %all-gather.3.cloned.1.call-update) | async-done | bytes 2621456 | tf_op jit(solution)/shard_map/all_gather | solution.py:33
  23.6 8.2 %convolution_convert_fusion = bf16[2560,1536]{1,0:T(8,128)(2,1)} fusion(bf16[2560,512]{1,0:T(8,128)(2,1)} %all-gather.3.cloned.1.call-done, bf16[1536,512]{1,0:T(8,128)(2,1)S(1)} %copy-done), kind=kOutput, calls=%fused_computation.15 | convolution fusion | flops 4030464000 | bytes 12058624 | tf_op jit(solution)/shard_map/dot_general | solution.py:16
  31.9 0.0 all-reduce.5.cloned.1.call-update
  31.9 0.0 all-gather.5.cloned.1.call-start
  32.0 0.7 all-gather.5.cloned.1.call-update
  32.6 0.0 all-reduce.7.cloned.1.call-start
  32.7 10.0 %fusion.14 = bf16[1536,512]{1,0:T(8,128)(2,1)} fusion(bf16[2560,512]{1,0:T(8,128)(2,1)} %all-gather.3.cloned.1.call-done, bf16[2560,1536]{1,0:T(8,128)(2,1)} %param.10, bf16[2560,1536]{1,0:T(8,128)(2,1)} %param.9), kind=kOutput, calls=%fused_computation.24 | convolution fusion | flops 4059561984 | bytes 19922944 | tf_op jit(solution)/shard_map/dot_general | solution.py:10
  42.7 264.3 %all-reduce.5.cloned.1.call-done = bf16[2560,1536]{1,0:T(8,128)(2,1)} async-done(((bf16[2560,1536]{1,0:T(8,128)(2,1)}), bf16[2560,1536]{1,0:T(8,128)(2,1)}) %all-reduce.5.cloned.1.call-update) | async-done | bytes 7864336 | tf_op jit(solution)/shard_map/psum | solution.py:35
  307.0 17.0 %fusion = (bf16[2560,1536]{1,0:T(8,128)(2,1)}, bf16[2560,1536]{1,0:T(8,128)(2,1)}) fusion(bf16[2560,1536]{1,0:T(8,128)(2,1)} %all-reduce.5.cloned.1.call-done, bf16[2560,1536]{1,0:T(8,128)(2,1)} %param.9, bf16[2560,1536]{1,0:T(8,128)(2,1)} %param.10), kind=kLoop, calls=%fused_computation.6 | loop fusion | flops 62914560 | bytes 39321600 | tf_op jit(solution)/shard_map/convert_element_type | solution.py:46
  324.1 9.6 %fusion.20 = bf16[512,1536]{0,1:T(8,128)(2,1)} fusion(bf16[2560,1536]{1,0:T(8,128)(2,1)} %get-tuple-element.22, bf16[2560,512]{1,0:T(8,128)(2,1)} %all-gather.5.cloned.1.call-done), kind=kOutput, calls=%fused_computation.28 | convolution fusion | flops 4028104704 | bytes 12058624 | tf_op jit(solution)/shard_map/dot_general | solution.py:10
  333.6 5.4 %fusion.19 = bf16[512,1536]{0,1:T(8,128)(2,1)} fusion(bf16[2560,1536]{1,0:T(8,128)(2,1)S(1)} %copy-done.2, bf16[2560,512]{1,0:T(8,128)(2,1)S(1)} %copy-done.4), kind=kOutput, calls=%fused_computation.27 | convolution fusion | flops 4028104704 | bytes 12058624 | tf_op jit(solution)/shard_map/dot_general | solution.py:10
  339.0 0.2 reduce-scatter.2.cloned.1.call-start
  339.3 6.9 %fusion.22 = f32[2560,512]{1,0:T(8,128)S(1)} fusion(bf16[2560,1536]{1,0:T(8,128)(2,1)} %get-tuple-element.22, bf16[512,1536]{1,0:T(8,128)(2,1)S(1)} %copy-done.5), kind=kOutput, calls=%fused_computation.30 | convolution fusion | flops 4026531840 | bytes 14680064 | tf_op jit(solution)/shard_map/dot_general | solution.py:16
  346.2 9.2 %add_convert_fusion = bf16[2560,512]{1,0:T(8,128)(2,1)} fusion(f32[2560,512]{1,0:T(8,128)S(1)} %fusion.22, bf16[2560,1536]{1,0:T(8,128)(2,1)} %get-tuple-element.21, bf16[512,1536]{1,0:T(8,128)(2,1)S(1)} %copy-done.6), kind=kOutput, calls=%fused_computation.17 | convolution fusion | flops 4029153280 | bytes 17301504 | tf_op jit(solution)/shard_map/dot_general | solution.py:16
  355.4 94.9 %all-reduce.7.cloned.1.call-done = (bf16[512,1536]{0,1:T(8,128)(2,1)}, bf16[512,1536]{0,1:T(8,128)(2,1)}, bf16[1536,512]{1,0:T(8,128)(2,1)}) async-done(((bf16[512,1536]{0,1:T(8,128)(2,1)}, bf16[512,1536]{0,1:T(8,128)(2,1)}, bf16[1536,512]{1,0:T(8,128)(2,1)}), (bf16[512,1536]{0,1:T(8,128)(2,1)}, bf16[512,1536]{0,1:T(8,128)(2,1)}, bf16[1536,512]{1,0:T(8,128)(2,1)})) %all-reduce.7.cloned.1.call-update) | async-done | bytes 4718608 | tf_op jit(solution)/shard_map/psum | solution.py:60
  450.4 3.2 copy.14
  453.5 3.2 copy.15
  456.7 2.1 multiply_reduce_fusion.1
  458.8 3.0 all-reduce
  461.8 3.5 multiply_reduce_fusion
  465.3 12.4 %psum.55 = f32[1536]{0:T(1024)} all-reduce(f32[1536]{0:T(1024)S(1)} %get-tuple-element.19), channel_id=1, replica_groups=mesh['rep'=4,'fs'=2,'tp'=4] {'tp'}, use_global_device_ids=true, to_apply=%region_10.0 | all-reduce | flops 1536 | bytes 12288 | tf_op jit(solution)/shard_map/psum | solution.py:26
  (18 shorter events, 0.1 us)
Async XLA Ops:
  7.2 16.5 %copy-start = (bf16[1536,512]{1,0:T(8,128)(2,1)S(1)}, bf16[1536,512]{1,0:T(8,128)(2,1)}, u32[]{:S(2)}) copy-start(bf16[1536,512]{1,0:T(8,128)(2,1)} %param.13) | copy-start | bytes 4718596
  7.2 16.5 %all-gather.3.cloned.1.call-start = ((), (), s32[]{:S(2)}) async-start(), calls=%async_computation.1 | async-start | bytes 3932160 | tf_op jit(solution)/shard_map/all_gather | solution.py:33
  7.9 299.1 %all-reduce.5.cloned.1.call-start = ((), (), s32[]{:S(2)}) async-start(), calls=%async_computation.2 | async-start | bytes 15728640 | tf_op jit(solution)/shard_map/psum | solution.py:35
  31.9 292.1 %all-gather.5.cloned.1.call-start = ((), (), s32[]{:S(2)}) async-start(), calls=%async_computation.4 | async-start | bytes 3932160 | tf_op jit(solution)/shard_map/all_gather | solution.py:32
  32.6 417.7 %all-reduce.7.cloned.1.call-start = ((), (), s32[]{:S(2)}) async-start(), calls=%async_computation.5 | async-start | bytes 9437184 | tf_op jit(solution)/shard_map/psum | solution.py:60
  324.1 9.6 %copy-start.2 = (bf16[2560,1536]{1,0:T(8,128)(2,1)S(1)}, bf16[2560,1536]{1,0:T(8,128)(2,1)}, u32[]{:S(2)}) copy-start(bf16[2560,1536]{1,0:T(8,128)(2,1)} %get-tuple-element.21) | copy-start | bytes 23592964
  324.1 9.6 %copy-start.4 = (bf16[2560,512]{1,0:T(8,128)(2,1)S(1)}, bf16[2560,512]{1,0:T(8,128)(2,1)}, u32[]{:S(2)}) copy-start(bf16[2560,512]{1,0:T(8,128)(2,1)} %all-gather.5.cloned.1.call-done) | copy-start | bytes 7864324
  333.6 5.7 %copy-start.5 = (bf16[512,1536]{1,0:T(8,128)(2,1)S(1)}, bf16[512,1536]{1,0:T(8,128)(2,1)}, u32[]{:S(2)}) copy-start(bf16[512,1536]{1,0:T(8,128)(2,1)} %param.11) | copy-start | bytes 4718596
  339.0 7.1 %copy-start.6 = (bf16[512,1536]{1,0:T(8,128)(2,1)S(1)}, bf16[512,1536]{1,0:T(8,128)(2,1)}, u32[]{:S(2)}) copy-start(bf16[512,1536]{1,0:T(8,128)(2,1)} %param.12) | copy-start | bytes 4718596
  339.0 138.7 %reduce-scatter.2.cloned.1.call-start = ((), (), s32[]{:S(2)}) async-start(), calls=%async_computation.3 | async-start | bytes 3932160 | tf_op jit(solution)/shard_map/reduce_scatter | solution.py:47
  450.3 6.4 %copy-start.3 = (bf16[512,1536]{0,1:T(8,128)(2,1)S(1)}, bf16[512,1536]{0,1:T(8,128)(2,1)}, u32[]{:S(2)}) copy-start(bf16[512,1536]{0,1:T(8,128)(2,1)} %get-tuple-element.16) | copy-start | bytes 4718596
  453.5 24.2 %copy-start.1 = (bf16[1536,512]{1,0:T(8,128)(2,1)S(1)}, bf16[1536,512]{1,0:T(8,128)(2,1)}, u32[]{:S(2)}) copy-start(bf16[1536,512]{1,0:T(8,128)(2,1)} %param.13) | copy-start | bytes 4718596
Sparse Core Ops, SparseCore 0:
  9.5 14.0 all-gather.2
  32.0 274.9 all-reduce.4
  308.6 10.1 all-gather.4
  339.2 111.1 all-reduce.6
  453.0 10.4 reduce-scatter.1
where the time goes:
time: 485 us; the launch traced here: 484 us
  waiting for transfers between devices  376 us (78%)
  matrix products  49.3 us (10%)
  other arithmetic  22.6 us (5%)
  blocking collectives  15.4 us (3%)
  between operations  13.8 us (3%)
  local copies, waits for them, and re-layouts  6.41 us (1%)
    psum x1, waiting for transfers between devices, on_device(): lax.psum(contract_cols(group_cotangent, down_weight).astype(jnp.bfloat16)...  264 us
    psum x1, waiting for transfers between devices, on_device(): lax.psum(gate_grad.astype(jnp.bfloat16), 'rep').astype(jnp.float32)  94.9 us
    dot_general x3, matrix products, contract_rows(): lax.dot_general(left_side, right_side, (((0,), (0,)), ((), ())), preferre...  25 us
    dot_general x3, matrix products, contract_cols(): lax.dot_general(left_side, right_side, (((1,), (1,)), ((), ())), preferre...  24.3 us
    convert_element_type x1, other arithmetic, on_device(): up_delta = (hidden_grad * activated).astype(jnp.bfloat16)  17 us
    all_gather x1, waiting for transfers between devices, on_device(): lax.all_gather(cotangent, 'fs', axis=0, tiled=True)  15.7 us
    psum x1, blocking collectives, row_squares(): down_sq = lax.psum(down_sq, 'tp')  12.4 us
  transfers between devices with their start and end apart: 5, of which 3 were waited for; matrix products, arithmetic and copies ran while one was open for 11% of the time, Pallas kernels for 0%

commit v1 on v0

v1 whole, which is shorter than its diff:
```python
import functools
import math

import jax
import jax.numpy as jnp
from jax import lax
from jax.experimental import pallas as pl
from jax.experimental.pallas import tpu as pltpu
from jax.sharding import PartitionSpec as P

F32 = jnp.float32
BF16 = jnp.bfloat16
TOKEN_CHUNKS = 4


def dot(left, right, left_dim, right_dim):
    return lax.dot_general(
        left, right, (((left_dim,), (right_dim,)), ((), ())), preferred_element_type=F32
    )


def swap(value, axis, size, mask):
    return lax.ppermute(value, axis, [(i, i ^ mask) for i in range(size)])


def rotate(value, axis, size, shift):
    return lax.ppermute(value, axis, [(i, (i - shift) % size) for i in range(size)])


def down_kernel(scale, order_ref, *refs):
    *token_refs, gate_ref, up_ref, out_ref, acc_ref = refs
    part, step = pl.program_id(0), pl.program_id(1)

    @pl.when((part == 0) & (step == 0))
    def _():
        acc_ref[...] = jnp.zeros_like(acc_ref)

    gate = gate_ref[...].astype(F32)
    hidden = (gate * jax.nn.sigmoid(gate) * up_ref[...].astype(F32)).astype(BF16)
    for index, ref in enumerate(token_refs):

        @pl.when(part == index)
        def _(ref=ref):
            acc_ref[...] += dot(hidden, ref[...], 0, 0)

    @pl.when((part == len(token_refs) - 1) & (step == pl.num_programs(1) - 1))
    def _():
        out_ref[...] = acc_ref[...] * scale


def down_partial(order, parts, gate_pre, up_pre, scale, tile):
    tokens, width = parts[0].shape
    hidden = gate_pre.shape[1]
    steps = tokens // tile

    def part_spec(index):
        def place(part, step, order_ref):
            at = jnp.where(part == index, step, jnp.where(part < index, 0, steps - 1))
            return (at, 0)

        return pl.BlockSpec((tile, width), place)

    rows = pl.BlockSpec(
        (tile, hidden), lambda part, step, order_ref: (order_ref[part] * steps + step, 0)
    )
    return pl.pallas_call(
        functools.partial(down_kernel, scale),
        grid_spec=pltpu.PrefetchScalarGridSpec(
            num_scalar_prefetch=1,
            grid=(len(parts), steps),
            in_specs=[part_spec(index) for index in range(len(parts))] + [rows, rows],
            out_specs=pl.BlockSpec(
                (hidden, width), lambda part, step, order_ref: (0, 0),
                pipeline_mode=pl.Buffered(1),
            ),
            scratch_shapes=[pltpu.VMEM((hidden, width), F32)],
        ),
        out_shape=jax.ShapeDtypeStruct((hidden, width), F32),
        name="down_partial",
    )(order, *parts, gate_pre, up_pre)


def chunk_kernel(n_parts, n_blocks, scale, order_ref, block_ref, chunk_ref, *refs):
    refs = list(refs)
    cot_ref = refs.pop(0)
    weight_refs = [refs.pop(0) for _ in range(n_blocks - 1)]
    far_refs = [refs.pop(0) for _ in range(2)]
    token_refs = [refs.pop(0) for _ in range(n_parts)]
    gate_ref, up_ref, gate_w_ref, up_w_ref = [refs.pop(0) for _ in range(4)]
    gate_in_ref, up_in_ref, input_ref, gate_out_ref, up_out_ref = refs
    part, step = pl.program_id(0), pl.program_id(1)

    @pl.when((part == 0) & (step == 0))
    def _():
        gate_out_ref[...] = gate_in_ref[...]
        up_out_ref[...] = up_in_ref[...]

    n_tp = cot_ref.shape[0]
    width = weight_refs[0].shape[1]
    token = token_refs[0][...]
    for index in range(1, n_parts):
        token = jnp.where(part == index, token_refs[index][...], token)
    total = None
    for block in range(n_blocks):
        columns = pl.ds(pl.multiple_of(block_ref[block] * width, width), width)
        hidden_grad = None
        for t in range(n_tp):
            if block < n_blocks - 1:
                weight = weight_refs[block][t]
            else:
                half = n_tp // 2
                weight = far_refs[t // half][t % half]
            term = dot(cot_ref[t, 0], weight, 1, 1)
            hidden_grad = term if hidden_grad is None else hidden_grad + term
        gate = gate_ref[:, columns].astype(F32)
        up = up_ref[:, columns].astype(F32)
        sigmoid = jax.nn.sigmoid(gate)
        gate_delta = (hidden_grad * up * sigmoid * (1.0 + gate * (1.0 - sigmoid))).astype(BF16)
        up_delta = (hidden_grad * (gate * sigmoid)).astype(BF16)
        gate_out_ref[:, columns] += dot(token, gate_delta, 0, 0)
        up_out_ref[:, columns] += dot(token, up_delta, 0, 0)
        term = dot(gate_delta, gate_w_ref[:, columns], 1, 1)
        term = term + dot(up_delta, up_w_ref[:, columns], 1, 1)
        total = term if total is None else total + term
    input_ref[0] = total.astype(BF16)

    done = (part == n_parts - 1) & (step == pl.num_programs(1) - 1)

    @pl.when(done & (chunk_ref[1] == 1))
    def _():
        gate_out_ref[...] = gate_out_ref[...] * scale
        up_out_ref[...] = up_out_ref[...] * scale


def chunk_grads(
    order, blocks, cot, weights, far, tokens, gate_pre, up_pre, gate_w, up_w, sums,
    place, scale, tile,
):
    n_tp, n_fs, rows, features = cot.shape
    all_rows = gate_pre.shape[0] // n_fs
    hidden = gate_pre.shape[1]
    steps = rows // tile
    whole = pl.Buffered(1)

    def fixed(shape):
        return pl.BlockSpec(shape, lambda *_: (0,) * len(shape), pipeline_mode=whole)

    def token_spec(index):
        def place(part, step, order_ref, block_ref, chunk_ref):
            at = jnp.where(part == index, step, jnp.where(part < index, 0, steps - 1))
            return (chunk_ref[0] * steps + at, 0)

        return pl.BlockSpec((tile, features), place)

    pre = pl.BlockSpec(
        (tile, hidden),
        lambda part, step, order_ref, block_ref, chunk_ref: (
            order_ref[part] * (all_rows // tile) + chunk_ref[0] * steps + step, 0,
        ),
    )
    in_specs = [
        pl.BlockSpec(
            (n_tp, 1, tile, features),
            lambda part, step, order_ref, block_ref, chunk_ref: (0, order_ref[part], step, 0),
        )
    ]
    in_specs += [fixed(value.shape) for value in (*weights, *far)]
    in_specs += [token_spec(index) for index in range(len(tokens))]
    in_specs += [pre, pre, fixed(gate_w.shape), fixed(up_w.shape)]
    operands = [cot, *weights, *far, *tokens, gate_pre, up_pre, gate_w, up_w]
    aliases = {3 + len(operands): 1, 4 + len(operands): 2}
    in_specs += [fixed(value.shape) for value in sums]
    operands += list(sums)
    return pl.pallas_call(
        functools.partial(
            chunk_kernel, len(tokens), len(weights) + 1, scale
        ),
        grid_spec=pltpu.PrefetchScalarGridSpec(
            num_scalar_prefetch=3,
            grid=(len(tokens), steps),
            in_specs=in_specs,
            out_specs=[
                pl.BlockSpec(
                    (1, tile, features),
                    lambda part, step, order_ref, block_ref, chunk_ref: (part, step, 0),
                ),
                fixed(gate_w.shape),
                fixed(up_w.shape),
            ],
        ),
        out_shape=[
            jax.ShapeDtypeStruct((len(tokens), rows, features), BF16),
            jax.ShapeDtypeStruct(gate_w.shape, F32),
            jax.ShapeDtypeStruct(up_w.shape, F32),
        ],
        input_output_aliases=aliases,
        name="chunk_grads",
    )(order, blocks, place, *operands)


def half_of(value, bit, keep):
    size = value.shape[0] // 2
    at = bit if keep else 1 - bit
    return lax.dynamic_slice_in_dim(value, at * size, size, 0)


def reduce_part(value, place, size, masks):
    for mask in masks:
        bit = (place // mask) % 2
        got = swap(half_of(value, bit, False).astype(BF16), "rep", size, mask)
        value = half_of(value, bit, True) + got.astype(F32)
    return value.astype(BF16)


def spread_part(piece, place, size, masks):
    pieces = {0: piece}
    for mask in reversed(masks):
        pieces.update({key ^ mask: swap(got, "rep", size, mask) for key, got in pieces.items()})
    offsets = {}
    for key in pieces:
        owner = place ^ key
        at = 0
        for mask in masks:
            at = at * 2 + (owner // mask) % 2
        offsets[key] = at
    return pieces, offsets


def place_kernel(n_pieces, start_ref, *refs):
    pieces, (out_ref, square_ref) = refs[:n_pieces], refs[n_pieces:]
    column = pl.program_id(0)

    @pl.when(column == 0)
    def _():
        square_ref[...] = jnp.zeros_like(square_ref)

    for index, ref in enumerate(pieces):
        rows = ref.shape[0]
        at = pl.ds(pl.multiple_of(start_ref[index] * rows, rows), rows)
        value = ref[...].astype(F32)
        out_ref[at, :] = value
        square_ref[at, :] += jnp.sum(value * value, axis=1, keepdims=True)


def place_rows(starts, pieces, rows):
    columns = pieces[0].shape[1]
    block = min(columns, 512)
    out, squares = pl.pallas_call(
        functools.partial(place_kernel, len(pieces)),
        grid_spec=pltpu.PrefetchScalarGridSpec(
            num_scalar_prefetch=1,
            grid=(columns // block,),
            in_specs=[
                pl.BlockSpec((piece.shape[0], block), lambda c, start_ref: (0, c))
                for piece in pieces
            ],
            out_specs=[
                pl.BlockSpec((rows, block), lambda c, start_ref: (0, c)),
                pl.BlockSpec((rows, 1), lambda c, start_ref: (0, 0)),
            ],
        ),
        out_shape=[
            jax.ShapeDtypeStruct((rows, columns), F32),
            jax.ShapeDtypeStruct((rows, 1), F32),
        ],
        name="place_rows",
    )(starts, *pieces)
    return out, squares[:, 0]


def sum_over_rep(value, place, size):
    masks = [1 << bit for bit in range(size.bit_length() - 1)]
    rows = value.shape[0]
    count = len(masks)
    part_rows = rows // count
    pieces, starts = [], []
    for index in range(count):
        turned = masks[index:] + masks[:index]
        part = value[index * part_rows:(index + 1) * part_rows]
        owned = reduce_part(part, place, size, turned)
        got, offsets = spread_part(owned, place, size, turned)
        for key in got:
            pieces.append(got[key])
            starts.append(index * size + offsets[key])
    starts = jnp.stack(starts).astype(jnp.int32)
    return place_rows(starts, pieces, rows)


def on_device(layer_input, cotangent, gate_pre, up_pre, gate_weight, up_weight, down_weight):
    n_rep, n_fs, n_tp = lax.axis_size("rep"), lax.axis_size("fs"), lax.axis_size("tp")
    rep, fs = lax.axis_index("rep"), lax.axis_index("fs")
    rows, features = cotangent.shape
    scale = 1.0 / math.sqrt(gate_pre.shape[0] * n_rep)
    order = ((fs + jnp.arange(n_fs)) % n_fs).astype(jnp.int32)
    tile = rows // TOKEN_CHUNKS

    share = down_weight.shape[0] // n_rep
    own = lax.all_gather(
        lax.dynamic_slice_in_dim(down_weight, rep * share, share, 0), "tp", axis=0
    )
    half = n_tp // 2
    near_x, near_y = swap(own, "rep", n_rep, 1), swap(own, "rep", n_rep, 2)
    far = (swap(near_x[:half], "rep", n_rep, 2), swap(near_y[half:], "rep", n_rep, 1))
    weights = (own, near_x, near_y)
    blocks = jnp.stack([rep, rep ^ 1, rep ^ 2, rep ^ 3]).astype(jnp.int32)

    chunks = [
        lax.all_gather(
            cotangent[index * tile:(index + 1) * tile], ("tp", "fs"), axis=0
        ).reshape(n_tp, n_fs, tile, features)
        for index in range(TOKEN_CHUNKS)
    ]

    cot_parts = [cotangent] + [rotate(cotangent, "fs", n_fs, k) for k in range(1, n_fs)]
    token_parts = [layer_input] + [rotate(layer_input, "fs", n_fs, k) for k in range(1, n_fs)]
    down_grad = down_partial(order, cot_parts, gate_pre, up_pre, scale, tile)
    down_grad, down_sq = sum_over_rep(down_grad, rep, n_rep)
    down_sq = lax.psum(down_sq, "tp")

    sums = (jnp.zeros(gate_weight.shape, F32), jnp.zeros(up_weight.shape, F32))
    kept, sent = [], []
    for index in range(TOKEN_CHUNKS):
        last = index == TOKEN_CHUNKS - 1
        if last:
            sums, down_sq = lax.optimization_barrier((sums, down_sq))
        partial, *sums = chunk_grads(
            order, blocks, chunks[index], weights, far, token_parts, gate_pre, up_pre,
            gate_weight, up_weight, sums, jnp.array([index, int(last)], jnp.int32), scale, tile,
        )
        kept.append(partial[0])
        sent.append(partial[1:])
    gate_grad, gate_sq = sum_over_rep(sums[0], rep, n_rep)
    up_grad, up_sq = sum_over_rep(sums[1], rep, n_rep)

    input_grad = jnp.concatenate(kept, 0).astype(F32)
    sent = jnp.concatenate(sent, 1)
    for k in range(1, n_fs):
        input_grad = input_grad + rotate(sent[k - 1], "fs", n_fs, -k).astype(F32)
    input_grad = input_grad.astype(BF16)
    gate_sq, up_sq = lax.psum((gate_sq, up_sq), "fs")
    return (input_grad, gate_grad, up_grad, down_grad, gate_sq, up_sq, down_sq)


def solution(mesh):
    return jax.shard_map(
        on_device,
        mesh=mesh,
        in_specs=(
            P(("rep", "fs"), "tp"),
            P(("rep", "fs"), "tp"),
            P("rep", "fs"),
            P("rep", "fs"),
            P("tp", "fs"),
            P("tp", "fs"),
            P("fs", "tp"),
        ),
        out_specs=(
            P(("rep", "fs"), "tp"),
            P("tp", "fs"),
            P("tp", "fs"),
            P("fs", "tp"),
            P("tp"),
            P("tp"),
            P("fs"),
        ),
        check_vma=False,
    )
```

time: 485 us -> 343 us (0.71); the launches traced: 484 us -> 337 us
  waiting for transfers between devices: 376 us -> 91.2 us
  Pallas kernels: 0 us -> 134 us
  matrix products: 49.3 us -> 0 us
  starting transfers between devices: 0.38 us -> 45.6 us
  local copies, waits for them, and re-layouts: 6.41 us -> 26.8 us
  other arithmetic: 22.6 us -> 10.7 us
    psum x2 -> x0, waiting for transfers between devices: 359 us -> none  [the longest x1 264 us: on_device(): lax.psum(contract_cols(group_cotangent, down_weight).astype(jnp.bfloat16)...]
    pallas_call x0 -> x8, Pallas kernels: none -> 134 us  [the longest x4 100 us: chunk_grads(): pl.pallas_call(functools.partial(chunk_kernel, len(tokens), len(weights)...]
    ppermute x0 -> x37, waiting for transfers between devices: none -> 77.5 us  [the longest x34 75.4 us: swap(): return lax.ppermute(value, axis, [(i, i ^ mask) for i in range(size)])]
    dot_general x6 -> x0, matrix products: 49.3 us -> none  [the longest x3 25 us: contract_rows(): lax.dot_general(left_side, right_side, (((0,), (0,)), ((), ())), preferre...]
    ppermute x0 -> x37, starting transfers between devices: none -> 45.4 us  [the longest x34 44.7 us: swap(): return lax.ppermute(value, axis, [(i, i ^ mask) for i in range(size)])]
    convert_element_type x1 -> x7, other arithmetic: 17 us -> 3.25 us  [the longest x1 3 us: on_device(): input_grad = input_grad.astype(BF16)]
    slice x0 -> x5, local copies, waits for them, and re-layouts: none -> 11.1 us  [the longest x2 6.61 us: sum_over_rep(): part = value[index * part_rows:(index + 1) * part_rows]]
    reduce_sum x2 -> x0, other arithmetic: 5.55 us -> none  [the longest x1 3.49 us: row_squares(): down_sq = jnp.sum(down_grad * down_grad, axis=1)]
  transfers between devices with their start and end apart: 5 -> 42, of which waited for: 3 -> 17; matrix products, arithmetic and copies ran while one was open for 11% -> 7% of each run, Pallas kernels for 0% -> 32%
where the time goes in v1:
time: 343 us; the launch traced here: 337 us
  Pallas kernels  134 us (39%)
  waiting for transfers between devices  91.2 us (27%)
  starting transfers between devices  45.6 us (13%)
  local copies, waits for them, and re-layouts  26.8 us (8%)
  between operations  14.5 us (4%)
  blocking collectives  13.9 us (4%)
  other arithmetic  10.7 us (3%)
    pallas_call x4, Pallas kernels, chunk_grads(): pl.pallas_call(functools.partial(chunk_kernel, len(tokens), len(weights)...  100 us
    ppermute x34, waiting for transfers between devices, swap(): return lax.ppermute(value, axis, [(i, i ^ mask) for i in range(size)])  75.4 us
    ppermute x34, starting transfers between devices, swap(): return lax.ppermute(value, axis, [(i, i ^ mask) for i in range(size)])  44.7 us
    pallas_call x1, Pallas kernels, down_partial(): pl.pallas_call(functools.partial(down_kernel, scale), grid_spec=pltpu.Pre...  20 us
    pallas_call x3, Pallas kernels, place_rows(): pl.pallas_call(functools.partial(place_kernel, len(pieces)), grid_spec=pl...  14.1 us
    all_gather x1, waiting for transfers between devices, on_device(): lax.all_gather(lax.dynamic_slice_in_dim(down_weight, rep * share, share,...  11.8 us
    psum x1, blocking collectives, on_device(): down_sq = lax.psum(down_sq, 'tp')  10.8 us
  transfers between devices with their start and end apart: 42, of which 17 were waited for; matrix products, arithmetic and copies ran while one was open for 7% of the time, Pallas kernels for 32%

profile of v1, /device:TPU:0, one launch (start us, length us, event | category | flops | bytes accessed | tf_op | source)
XLA Modules:
  0.0 336.6 jit_solution(14789725387334383381)
XLA Ops:
  9.4 2.5 fusion.4
  14.9 2.1 collective-permute-done.5.refs_1_
  18.1 20.0 %down_partial.1 = f32[1536,512]{1,0:T(8,128)} custom-call(s32[2]{0:T(128)} %and_select_fusion.order_ref, bf16[1280,512]{1,0:T(8,128)(2,1)} %refs_0_.1, bf16[1280,512]{1,0:T(8,128)(2,1)} %copy-done.7, bf16[2560,1536]{1,0:T(8,128)(2,1)} %refs_8_.7, bf16[2560,1536]{1,0:T(8,128)(2,1)} %refs_9_.7), custom_call_target="tpu_custom_call" | custom-call | tf_op jit(solution)/shard_map/down_partial/pallas_call | solution.py:66
  38.1 11.8 %all-gather.13.cloned.1.call-done = bf16[1536,512]{1,0:T(8,128)(2,1)} async-done(((bf16[384,512]{1,0:T(8,128)(2,1)}), bf16[1536,512]{1,0:T(8,128)(2,1)}) %all-gather.13.cloned.1.call-update) | async-done | bytes 1572880 | tf_op jit(solution)/shard_map/all_gather | solution.py:298
  52.9 3.3 fusion.3
  61.2 33.8 %collective-permute-done.11 = bf16[384,512]{1,0:T(8,128)(2,1)S(1)} collective-permute-done((bf16[384,512]{1,0:T(8,128)(2,1)}, bf16[384,512]{1,0:T(8,128)(2,1)S(1)}, u32[]{:S(2)}, u32[]{:S(2)}) %collective-permute-start.11) | collective-permute-done | bytes 393248 | tf_op jit(solution)/shard_map/ppermute | solution.py:23
  107.4 15.7 %collective-permute-done.13.refs_5_ = bf16[192,512]{1,0:T(8,128)(2,1)S(1)} collective-permute-done((bf16[192,512]{1,0:T(8,128)(2,1)S(1)}, bf16[192,512]{1,0:T(8,128)(2,1)S(1)}, u32[]{:S(2)}, u32[]{:S(2)}) %collective-permute-start.13) | collective-permute-done | bytes 196640 | tf_op jit(solution)/shard_map/ppermute | solution.py:23
  130.9 2.7 collective-permute-done.9.refs_2_
  136.3 3.0 collective-permute-done.10.refs_3_
  140.0 4.4 %place_rows.3 = (f32[1536,512]{1,0:T(8,128)}, f32[1536,1]{1,0:T(8,128)}) custom-call(s32[8]{0:T(128)} %stack.73.start_ref, bf16[192,512]{1,0:T(8,128)(2,1)} %copy-done.9, bf16[192,512]{1,0:T(8,128)(2,1)} %copy-done.20, bf16[192,512]{1,0:T(8,128)(2,1)} %copy-done.21, bf16[192,512]{1,0:T(8,128)(2,1)} %copy-done.23, bf16[192,512]{1,0:T(8,128)(2,1)} %copy-done.8, ...), custom_call_target="tpu_custom_call" | custom-call | tf_op jit(solution)/shard_map/place_rows/pallas_call | solution.py:248
  145.9 10.8 %psum.21 = f32[1536]{0:T(1024)} all-reduce(f32[1536]{0:T(1024)S(1)} %reduce), channel_id=1, replica_groups=mesh['rep'=4,'fs'=2,'tp'=4] {'tp'}, use_global_device_ids=true, to_apply=%region_0.1 | all-reduce | flops 1536 | bytes 12288 | tf_op jit(solution)/shard_map/psum | solution.py:318
  161.3 24.6 %chunk_grads.4 = (bf16[2,320,512]{2,1,0:T(8,128)(2,1)}, f32[512,1536]{1,0:T(8,128)}, f32[512,1536]{1,0:T(8,128)}) custom-call(s32[2]{0:T(128)} %and_select_fusion.order_ref, s32[4]{0:T(128)} %pad_add_fusion.block_ref, s32[2]{0:T(128)} %broadcast.25.chunk_ref, bf16[4,2,320,512]{3,2,1,0:T(8,128)(2,1)} %bitcast.36, ...), custom_call_target="tpu_custom_call", output_to_operand_aliasing={{1}: (15, {}), {2}: (16, {})} | custom-call | tf_op jit(solution)/shard_map/chunk_grads/pallas_call | solution.py:174
  186.0 25.1 %chunk_grads.5 = (bf16[2,320,512]{2,1,0:T(8,128)(2,1)}, f32[512,1536]{1,0:T(8,128)}, f32[512,1536]{1,0:T(8,128)}) custom-call(s32[2]{0:T(128)} %and_select_fusion.order_ref, s32[4]{0:T(128)} %pad_add_fusion.block_ref, s32[2]{0:T(128)} %constant.359.clone.chunk_ref, ...), custom_call_target="tpu_custom_call", output_to_operand_aliasing={{1}: (15, {}), {2}: (16, {})} | custom-call | tf_op jit(solution)/shard_map/chunk_grads/pallas_call | solution.py:174
  211.2 24.8 %chunk_grads.6 = (bf16[2,320,512]{2,1,0:T(8,128)(2,1)}, f32[512,1536]{1,0:T(8,128)}, f32[512,1536]{1,0:T(8,128)}) custom-call(s32[2]{0:T(128)} %and_select_fusion.order_ref, s32[4]{0:T(128)} %pad_add_fusion.block_ref, s32[2]{0:T(128)} %constant.360.clone.chunk_ref, ...), custom_call_target="tpu_custom_call", output_to_operand_aliasing={{1}: (15, {}), {2}: (16, {})} | custom-call | tf_op jit(solution)/shard_map/chunk_grads/pallas_call | solution.py:174
  236.0 25.4 %chunk_grads.7 = (bf16[2,320,512]{2,1,0:T(8,128)(2,1)}, f32[512,1536]{1,0:T(8,128)}, f32[512,1536]{1,0:T(8,128)}) custom-call(s32[2]{0:T(128)} %and_select_fusion.order_ref, s32[4]{0:T(128)} %pad_add_fusion.block_ref, s32[2]{0:T(128)} %constant.361.clone.chunk_ref, ...), custom_call_target="tpu_custom_call", output_to_operand_aliasing={{1}: (15, {}), {2}: (16, {})} | custom-call | tf_op jit(solution)/shard_map/chunk_grads/pallas_call | solution.py:174
  261.4 3.3 fusion.1
  271.0 3.9 %collective-permute-done.32 = bf16[128,1536]{1,0:T(8,128)(2,1)S(1)} collective-permute-done((bf16[128,1536]{1,0:T(8,128)(2,1)S(1)}, bf16[128,1536]{1,0:T(8,128)(2,1)S(1)}, u32[]{:S(2)}, u32[]{:S(2)}) %collective-permute-start.32) | collective-permute-done | bytes 393248 | tf_op jit(solution)/shard_map/ppermute | solution.py:23
  278.4 4.6 %collective-permute-done.22 = bf16[128,1536]{1,0:T(8,128)(2,1)S(1)} collective-permute-done((bf16[128,1536]{1,0:T(8,128)(2,1)S(1)}, bf16[128,1536]{1,0:T(8,128)(2,1)S(1)}, u32[]{:S(2)}, u32[]{:S(2)}) %collective-permute-start.22) | collective-permute-done | bytes 393248 | tf_op jit(solution)/shard_map/ppermute | solution.py:23
  286.8 2.4 collective-permute-done.33
  305.0 2.1 collective-permute-done.24.refs_5_
  311.9 4.8 %place_rows.5 = (f32[512,1536]{1,0:T(8,128)}, f32[512,1]{1,0:T(8,128)}) custom-call(s32[8]{0:T(128)} %stack.73.start_ref, bf16[64,1536]{1,0:T(8,128)(2,1)} %copy-done.13, bf16[64,1536]{1,0:T(8,128)(2,1)} %copy-done.27, bf16[64,1536]{1,0:T(8,128)(2,1)} %copy-done.28, bf16[64,1536]{1,0:T(8,128)(2,1)} %copy-done.30, bf16[64,1536]{1,0:T(8,128)(2,1)} %copy-done.10, ...), custom_call_target="tpu_custom_call" | custom-call | tf_op jit(solution)/shard_map/place_rows/pallas_call | solution.py:248
  317.9 4.8 %place_rows.4 = (f32[512,1536]{1,0:T(8,128)}, f32[512,1]{1,0:T(8,128)}) custom-call(s32[8]{0:T(128)} %stack.73.start_ref, bf16[64,1536]{1,0:T(8,128)(2,1)} %copy-done.12, bf16[64,1536]{1,0:T(8,128)(2,1)} %collective-permute-done.19.refs_1_, bf16[64,1536]{1,0:T(8,128)(2,1)} %collective-permute-done.20.refs_2_, ...), custom_call_target="tpu_custom_call" | custom-call | tf_op jit(solution)/shard_map/place_rows/pallas_call | solution.py:248
  323.8 3.0 all-reduce
  326.9 3.0 add_convert_fusion
  (180 shorter events, 80.0 us)
Async XLA Ops:
  7.2 42.7 %all-gather.13.cloned.1.call-start = ((), (), s32[]{:S(2)}) async-start(), calls=%async_computation.1 | async-start | bytes 1966080 | tf_op jit(solution)/shard_map/all_gather | solution.py:298
  9.4 147.3 %all-gather.11.cloned.1.call-start = ((), (), s32[]{:S(2)}) async-start(), calls=%async_computation | async-start | bytes 2949120 | tf_op jit(solution)/shard_map/all_gather | solution.py:308
  11.9 174.1 %all-gather.15.cloned.1.call-start = ((), (), s32[]{:S(2)}) async-start(), calls=%async_computation.2 | async-start | bytes 2949120 | tf_op jit(solution)/shard_map/all_gather | solution.py:308
  12.7 198.5 %all-gather.17.cloned.1.call-start = ((), (), s32[]{:S(2)}) async-start(), calls=%async_computation.3 | async-start | bytes 2949120 | tf_op jit(solution)/shard_map/all_gather | solution.py:308
  13.3 222.8 %all-gather.19.cloned.1.call-start = ((), (), s32[]{:S(2)}) async-start(), calls=%async_computation.4 | async-start | bytes 2949120 | tf_op jit(solution)/shard_map/all_gather | solution.py:308
  49.9 49.7 %collective-permute-start = (bf16[4,384,512]{2,1,0:T(8,128)(2,1)}, bf16[4,384,512]{2,1,0:T(8,128)(2,1)S(1)}, u32[]{:S(2)}, u32[]{:S(2)}) collective-permute-start(bf16[4,384,512]{2,1,0:T(8,128)(2,1)} %bitcast.27), channel_id=1, source_target_pairs={{0,8},{8,0},{16,24},{24,16},{1,9},{9,1},{17,25},{25,17},{2,10},{10... | collective-permute-start | bytes 4718600 | tf_op jit(solution)/shard_map/ppermute | solution.py:23
  51.4 49.8 %collective-permute-start.1 = (bf16[4,384,512]{2,1,0:T(8,128)(2,1)}, bf16[4,384,512]{2,1,0:T(8,128)(2,1)S(1)}, u32[]{:S(2)}, u32[]{:S(2)}) collective-permute-start(bf16[4,384,512]{2,1,0:T(8,128)(2,1)} %bitcast.28), channel_id=1, source_target_pairs={{0,16},{8,24},{16,0},{24,8},{1,17},{9,25},{17,1},{25,9},{2,18},{10... | collective-permute-start | bytes 4718600 | tf_op jit(solution)/shard_map/ppermute | solution.py:23
  58.1 36.9 %collective-permute-start.11 = (bf16[384,512]{1,0:T(8,128)(2,1)}, bf16[384,512]{1,0:T(8,128)(2,1)S(1)}, u32[]{:S(2)}, u32[]{:S(2)}) collective-permute-start(bf16[384,512]{1,0:T(8,128)(2,1)} %dynamic-slice_convert_fusion.4), channel_id=1, source_target_pairs={{0,16},{8,24},{16,0},{24,8},{1,17},{9,25},{17,1},{25,9},{2,18},{10... | collective-permute-start | bytes 1179656 | tf_op jit(solution)/shard_map/ppermute | solution.py:23
  60.6 36.3 %collective-permute-start.6 = (bf16[384,512]{1,0:T(8,128)(2,1)}, bf16[384,512]{1,0:T(8,128)(2,1)}, u32[]{:S(2)}, u32[]{:S(2)}) collective-permute-start(bf16[384,512]{1,0:T(8,128)(2,1)} %dynamic-slice_convert_fusion.5), channel_id=1, source_target_pairs={{0,8},{8,0},{16,24},{24,16},{1,9},{9,1},{17,25},{25,17},{2,10},{10... | collective-permute-start | bytes 1179656 | tf_op jit(solution)/shard_map/ppermute | solution.py:23
  61.2 95.5 %collective-permute-start.4 = (bf16[1280,512]{1,0:T(8,128)(2,1)}, bf16[1280,512]{1,0:T(8,128)(2,1)}, u32[]{:S(2)}, u32[]{:S(2)}) collective-permute-start(bf16[1280,512]{1,0:T(8,128)(2,1)} %refs_6_.7), channel_id=1, source_target_pairs={{0,4},{4,0},{1,5},{5,1},{2,6},{6,2},{3,7},{7,3},{8,12},{12,8},{9,1... | collective-permute-start | bytes 3932168 | tf_op jit(solution)/shard_map/ppermute | solution.py:27
  100.6 56.1 %collective-permute-start.2 = (bf16[2,384,512]{2,1,0:T(8,128)(2,1)}, bf16[2,384,512]{2,1,0:T(8,128)(2,1)}, u32[]{:S(2)}, u32[]{:S(2)}) collective-permute-start(bf16[2,384,512]{2,1,0:T(8,128)(2,1)} %slice.80), channel_id=1, source_target_pairs={{0,16},{8,24},{16,0},{24,8},{1,17},{9,25},{17,1},{25,9},{2,18},{10... | collective-permute-start | bytes 2359304 | tf_op jit(solution)/shard_map/ppermute | solution.py:23
  102.2 54.6 %collective-permute-start.3 = (bf16[2,384,512]{2,1,0:T(8,128)(2,1)}, bf16[2,384,512]{2,1,0:T(8,128)(2,1)}, u32[]{:S(2)}, u32[]{:S(2)}) collective-permute-start(bf16[2,384,512]{2,1,0:T(8,128)(2,1)} %slice.81), channel_id=1, source_target_pairs={{0,8},{8,0},{16,24},{24,16},{1,9},{9,1},{17,25},{25,17},{2,10},{10... | collective-permute-start | bytes 2359304 | tf_op jit(solution)/shard_map/ppermute | solution.py:23
  103.7 19.5 %collective-permute-start.13 = (bf16[192,512]{1,0:T(8,128)(2,1)S(1)}, bf16[192,512]{1,0:T(8,128)(2,1)S(1)}, u32[]{:S(2)}, u32[]{:S(2)}) collective-permute-start(bf16[192,512]{1,0:T(8,128)(2,1)S(1)} %add_convert_fusion.5.refs_4_), channel_id=1, source_target_pairs={{0,8},{8,0},{16,24},{24,16},{1,9},{9,1},{17,25},{25,17},{2,10},{10... | collective-permute-start | bytes 589832 | tf_op jit(solution)/shard_map/ppermute | solution.py:23
  105.9 20.0 %collective-permute-start.14 = (bf16[192,512]{1,0:T(8,128)(2,1)S(1)}, bf16[192,512]{1,0:T(8,128)(2,1)S(1)}, u32[]{:S(2)}, u32[]{:S(2)}) collective-permute-start(bf16[192,512]{1,0:T(8,128)(2,1)S(1)} %add_convert_fusion.5.refs_4_), channel_id=1, source_target_pairs={{0,16},{8,24},{16,0},{24,8},{1,17},{9,25},{17,1},{25,9},{2,18},{10... | collective-permute-start | bytes 589832 | tf_op jit(solution)/shard_map/ppermute | solution.py:23
  264.8 10.1 %collective-permute-start.32 = (bf16[128,1536]{1,0:T(8,128)(2,1)S(1)}, bf16[128,1536]{1,0:T(8,128)(2,1)S(1)}, u32[]{:S(2)}, u32[]{:S(2)}) collective-permute-start(bf16[128,1536]{1,0:T(8,128)(2,1)S(1)} %dynamic-slice_convert_fusion), channel_id=1, source_target_pairs={{0,16},{8,24},{16,0},{24,8},{1,17},{9,25},{17,1},{25,9},{2,18},{10... | collective-permute-start | bytes 1179656 | tf_op jit(solution)/shard_map/ppermute | solution.py:23
  266.2 10.3 %collective-permute-start.27 = (bf16[128,1536]{1,0:T(8,128)(2,1)S(1)}, bf16[128,1536]{1,0:T(8,128)(2,1)S(1)}, u32[]{:S(2)}, u32[]{:S(2)}) collective-permute-start(bf16[128,1536]{1,0:T(8,128)(2,1)S(1)} %dynamic-slice_convert_fusion.1), channel_id=1, source_target_pairs={{0,8},{8,0},{16,24},{24,16},{1,9},{9,1},{17,25},{25,17},{2,10},{10... | collective-permute-start | bytes 1179656 | tf_op jit(solution)/shard_map/ppermute | solution.py:23
  267.5 15.4 %collective-permute-start.22 = (bf16[128,1536]{1,0:T(8,128)(2,1)S(1)}, bf16[128,1536]{1,0:T(8,128)(2,1)S(1)}, u32[]{:S(2)}, u32[]{:S(2)}) collective-permute-start(bf16[128,1536]{1,0:T(8,128)(2,1)S(1)} %dynamic-slice_convert_fusion.2), channel_id=1, source_target_pairs={{0,16},{8,24},{16,0},{24,8},{1,17},{9,25},{17,1},{25,9},{2,18},{10... | collective-permute-start | bytes 1179656 | tf_op jit(solution)/shard_map/ppermute | solution.py:23
  268.7 16.4 %collective-permute-start.17 = (bf16[128,1536]{1,0:T(8,128)(2,1)S(1)}, bf16[128,1536]{1,0:T(8,128)(2,1)S(1)}, u32[]{:S(2)}, u32[]{:S(2)}) collective-permute-start(bf16[128,1536]{1,0:T(8,128)(2,1)S(1)} %dynamic-slice_convert_fusion.3), channel_id=1, source_target_pairs={{0,8},{8,0},{16,24},{24,16},{1,9},{9,1},{17,25},{25,17},{2,10},{10... | collective-permute-start | bytes 1179656 | tf_op jit(solution)/shard_map/ppermute | solution.py:23
  270.9 56.0 %collective-permute-start.16 = (bf16[1280,512]{1,0:T(8,128)(2,1)S(1)}, bf16[1280,512]{1,0:T(8,128)(2,1)}, u32[]{:S(2)}, u32[]{:S(2)}) collective-permute-start(bf16[1280,512]{1,0:T(8,128)(2,1)S(1)} %maximum_bitcast_fusion), channel_id=1, source_target_pairs={{0,4},{4,0},{1,5},{5,1},{2,6},{6,2},{3,7},{7,3},{8,12},{12,8},{9,1... | collective-permute-start | bytes 3932168 | tf_op jit(solution)/shard_map/ppermute | solution.py:27
  275.0 14.2 %collective-permute-start.33 = (bf16[64,1536]{1,0:T(8,128)(2,1)S(1)}, bf16[64,1536]{1,0:T(8,128)(2,1)S(1)}, u32[]{:S(2)}, u32[]{:S(2)}) collective-permute-start(bf16[64,1536]{1,0:T(8,128)(2,1)S(1)} %dynamic-slice_convert_fusion.6), channel_id=1, source_target_pairs={{0,8},{8,0},{16,24},{24,16},{1,9},{9,1},{17,25},{25,17},{2,10},{10... | collective-permute-start | bytes 589832 | tf_op jit(solution)/shard_map/ppermute | solution.py:23
  276.7 14.2 %collective-permute-start.28 = (bf16[64,1536]{1,0:T(8,128)(2,1)S(1)}, bf16[64,1536]{1,0:T(8,128)(2,1)S(1)}, u32[]{:S(2)}, u32[]{:S(2)}) collective-permute-start(bf16[64,1536]{1,0:T(8,128)(2,1)S(1)} %dynamic-slice_convert_fusion.7), channel_id=1, source_target_pairs={{0,16},{8,24},{16,0},{24,8},{1,17},{9,25},{17,1},{25,9},{2,18},{10... | collective-permute-start | bytes 589832 | tf_op jit(solution)/shard_map/ppermute | solution.py:23
  283.1 10.4 %collective-permute-start.23 = (bf16[64,1536]{1,0:T(8,128)(2,1)S(1)}, bf16[64,1536]{1,0:T(8,128)(2,1)S(1)}, u32[]{:S(2)}, u32[]{:S(2)}) collective-permute-start(bf16[64,1536]{1,0:T(8,128)(2,1)S(1)} %dynamic-slice_convert_fusion.8), channel_id=1, source_target_pairs={{0,8},{8,0},{16,24},{24,16},{1,9},{9,1},{17,25},{25,17},{2,10},{10... | collective-permute-start | bytes 589832 | tf_op jit(solution)/shard_map/ppermute | solution.py:23
  307.1 10.8 %collective-permute-start.25 = (bf16[64,1536]{1,0:T(8,128)(2,1)S(1)}, bf16[64,1536]{1,0:T(8,128)(2,1)}, u32[]{:S(2)}, u32[]{:S(2)}) collective-permute-start(bf16[64,1536]{1,0:T(8,128)(2,1)S(1)} %add_convert_fusion.3.refs_4_), channel_id=1, source_target_pairs={{0,16},{8,24},{16,0},{24,8},{1,17},{9,25},{17,1},{25,9},{2,18},{10... | collective-permute-start | bytes 589832 | tf_op jit(solution)/shard_map/ppermute | solution.py:23
  307.7 10.2 %collective-permute-start.20 = (bf16[64,1536]{1,0:T(8,128)(2,1)S(1)}, bf16[64,1536]{1,0:T(8,128)(2,1)}, u32[]{:S(2)}, u32[]{:S(2)}) collective-permute-start(bf16[64,1536]{1,0:T(8,128)(2,1)S(1)} %add_convert_fusion.4.refs_0_), channel_id=1, source_target_pairs={{0,8},{8,0},{16,24},{24,16},{1,9},{9,1},{17,25},{25,17},{2,10},{10... | collective-permute-start | bytes 589832 | tf_op jit(solution)/shard_map/ppermute | solution.py:23
  (49 other events, 461.6 us)
Sparse Core Ops, SparseCore 0:
  10.1 39.7 all-gather.12
  51.6 32.5 all-gather.10
  85.8 32.8 all-gather.14
  120.2 33.2 all-gather.16
  154.9 32.7 all-gather.18
